TPU v7x, 128 devices: a whole 4x4x4 slice. The times are simulated.
128 devices in a mesh: rep: 2 (over z_hi), fs: 32 (over z_lo, y, x), tp: 2 (over core).
Axes of the slice: x: 4, y: 4, z: 4 (z_hi: 2, z_lo: 2; z = z_hi * 2 + z_lo), core: 2. Of those that a mesh axis runs over, the one named last changes fastest.
Arguments:
- hidden_in: bfloat16 [40960, 2048], P(('rep', 'fs'), 'tp'), may hold values from -6 to 6
- mix_gain: float32 [2048], replicated, may hold values from 0.1 to 1.9
- w_value: bfloat16 [2048, 1024], P('fs', 'tp'), may hold values from -0.125 to 0.125
- w_gate: bfloat16 [2048, 1024], P('fs', 'tp'), may hold values from -0.125 to 0.125
- conv_taps: float32 [31, 1024], P(None, 'tp'), may hold values from -5 to 5
- conv_bias: float32 [1024], P('tp'), may hold values from -3 to 3
- chan_gain: float32 [1024], P('tp'), may hold values from 0.1 to 1.9
- chan_bias: float32 [1024], P('tp'), may hold values from -3 to 3
- w_back: bfloat16 [1024, 2048], P('tp', 'fs'), may hold values from -0.1875 to 0.1875
- feed_gain: float32 [2048], replicated, may hold values from 0.1 to 1.9
- w_up: bfloat16 [2048, 8192], P(None, ('fs', 'tp')), may hold values from -0.125 to 0.125
- w_down: bfloat16 [8192, 2048], P(('fs', 'tp')), may hold values from -0.0625 to 0.0625
Outputs:
- layer_out: bfloat16 [40960, 2048], P(('rep', 'fs'), 'tp')
All inputs are finite; a program needn't handle non-finite values.
Results may differ from a plain program's by a relative error of at most 0.015.
Values may be sent and summed in bfloat16 or wider, within the bound.
A program may use at most 128 MiB of HBM per device.

v0:
```python
import jax
import jax.numpy as jnp
from jax import lax
from jax.sharding import PartitionSpec as P

KW = 31
LEN = 128


def copy_for_each(array, axis):
    copies = jnp.broadcast_to(array, (lax.axis_size(axis), *array.shape))
    return lax.all_to_all(copies, axis, split_axis=0, concat_axis=0, tiled=True)


def in_order(parts, dim):
    lengths = list(parts.shape[1:])
    lengths[dim] *= parts.shape[0]
    return jnp.moveaxis(parts, 0, dim).reshape(lengths)


def gathered_copies(array, axis, dim):
    parts = copy_for_each(array, axis)
    return in_order(parts, dim)


def side_by_side(arrays, axis, dim, along):
    widths = [a.shape[along] for a in arrays]
    both = jnp.concatenate(arrays, axis=along)
    result = lax.all_gather(both, axis, axis=dim, tiled=True)
    return tuple(jnp.split(result, [sum(widths[:k]) for k in range(1, len(widths))], axis=along))


def in_blocks(array, dim, count):
    lengths = array.shape
    parts = array.reshape(*lengths[:dim], count, lengths[dim] // count, *lengths[dim + 1 :])
    return jnp.moveaxis(parts, dim, 0)


def summed_on_arrival(array, axis, dim):
    count = lax.axis_size(axis)
    parts = lax.all_to_all(in_blocks(array, dim, count), axis, 0, 0, tiled=True)
    return jnp.sum(parts.astype(jnp.float32), axis=0)


def rms_norm(stream, gain):
    values = stream.astype(jnp.float32)
    scaled = values * lax.rsqrt(jnp.mean(values * values, axis=-1, keepdims=True) + 1e-06)
    return (scaled * gain).astype(jnp.bfloat16)


def causal_filter(gated, conv_taps, conv_bias):
    channels = gated.shape[1]
    blocks = gated.reshape(gated.shape[0] // LEN, LEN, channels)
    padded = jnp.pad(blocks, ((0, 0), (KW - 1, 0), (0, 0)))
    result = jnp.zeros_like(blocks) + conv_bias
    for tap_index in range(KW):
        result = result + conv_taps[tap_index] * padded[:, tap_index : tap_index + LEN]
    return result.reshape(gated.shape)


def shards(
    hidden_in,
    mix_gain,
    w_value,
    w_gate,
    conv_taps,
    conv_bias,
    chan_gain,
    chan_bias,
    w_back,
    feed_gain,
    w_up,
    w_down,
):
    gathered = gathered_copies(hidden_in, "tp", 1)
    normed = rms_norm(gathered, mix_gain)
    local_channels = w_value.shape[1]
    whole_value, whole_gate = side_by_side((w_value, w_gate), "fs", 0, 1)
    value_proj = jnp.dot(normed, whole_value, preferred_element_type=jnp.float32)
    gate_proj = jnp.dot(normed, whole_gate, preferred_element_type=jnp.float32)
    gated = value_proj * jax.nn.sigmoid(gate_proj)
    filtered = causal_filter(gated, conv_taps, conv_bias)
    channel_total = local_channels * lax.axis_size("tp")
    first_sum, square_sum = lax.psum(
        (jnp.sum(filtered, axis=1), jnp.sum(filtered * filtered, axis=1)), "tp"
    )
    chan_mean = (first_sum / channel_total)[:, None]
    chan_var = (square_sum / channel_total)[:, None] - chan_mean * chan_mean
    centred = (filtered - chan_mean) * lax.rsqrt(chan_var + 1e-05) * chan_gain + chan_bias
    mixer_act = jax.nn.silu(centred).astype(jnp.bfloat16)
    whole_back = gathered_copies(w_back, "fs", 1)
    partial_value = jnp.dot(mixer_act, whole_back, preferred_element_type=jnp.float32)
    summed = summed_on_arrival(partial_value.astype(jnp.bfloat16), "tp", 1)
    second = (hidden_in.astype(jnp.float32) + summed).astype(jnp.bfloat16)
    gathered_feed = lax.all_gather(second, "tp", axis=1, tiled=True)
    normed_feed = rms_norm(gathered_feed, feed_gain)
    up_proj = jnp.dot(
        normed_feed,
        lax.all_gather(w_up, "fs", axis=1, tiled=True),
        preferred_element_type=jnp.float32,
    )
    hidden = jnp.square(jax.nn.relu(up_proj)).astype(jnp.bfloat16)
    feed_partial = jnp.dot(
        hidden, lax.all_gather(w_down, "fs", axis=0, tiled=True), preferred_element_type=jnp.float32
    )
    feed = summed_on_arrival(feed_partial.astype(jnp.bfloat16), "tp", 1)
    return (second.astype(jnp.float32) + feed).astype(jnp.bfloat16)


def solution(mesh):
    placed = (
        P(("rep", "fs"), "tp"),
        P(),
        P("fs", "tp"),
        P("fs", "tp"),
        P(None, "tp"),
        P("tp"),
        P("tp"),
        P("tp"),
        P("tp", "fs"),
        P(),
        P(None, ("fs", "tp")),
        P(("fs", "tp"), None),
    )
    return jax.shard_map(
        shards, mesh=mesh, in_specs=placed, out_specs=P(("rep", "fs"), "tp"), check_vma=False
    )
```

profile of v0, /device:TPU:1, one launch (start us, length us, event | category | flops | bytes accessed | tf_op | source)
XLA Modules:
  0.0 708.8 jit_solution(11881618682649393780)
XLA Ops:
  6.5 0.0 all-gather.5.cloned.1.call-start
  6.5 1.5 pad_maximum_fusion
  8.1 0.0 all-gather.5.cloned.1.call-update
  8.1 1.7 copy.15
  9.8 0.2 broadcast_in_dim.4
  10.0 0.0 copy-start.5
  10.0 7.0 all_to_all.20
  17.0 0.0 copy-done.5
  17.0 1.6 broadcast_in_dim.5
  18.6 8.6 %all-to-all-start.1 = ((bf16[32,512,64]{1,2,0:T(8,128)(2,1)}), bf16[32,512,64]{1,2,0:T(8,128)(2,1)}, u32[]{:S(2)}, u32[]{:S(2)}) async-start(bf16[32,512,64]{1,2,0:T(8,128)(2,1)} %broadcast_in_dim.5), calls=%async_computation.1 | async-start | bytes 4194304 | tf_op jit(solution)/shard_map/all_to_all | solution.py:12
  27.3 0.0 copy-start.6
  27.3 0.0 copy-start.7
  27.3 0.0 all-gather.7.cloned.1.call-start
  27.3 0.6 multiply_reduce_fusion
  27.9 0.2 copy-done.6
  28.2 0.0 copy-done.7
  28.2 2.2 fusion.4
  30.4 0.0 copy-start.1
  30.4 127.4 %all-gather.5.cloned.1.call-done = bf16[2048,1024]{1,0:T(8,128)(2,1)} async-done(((bf16[64,1024]{1,0:T(8,128)(2,1)}), bf16[2048,1024]{1,0:T(8,128)(2,1)}) %all-gather.5.cloned.1.call-update) | async-done | bytes 4194320 | tf_op jit(solution)/shard_map/all_gather | solution.py:29
  157.8 0.0 copy-start.4
  157.8 4.2 fusion.28
  162.0 0.0 copy-done.1
  162.0 0.0 copy-done.4
  162.0 0.0 copy-start.8
  162.1 1.6 fusion.16
  163.6 0.0 copy-done.8
  163.7 0.0 copy-start.9
  163.7 0.0 copy-start.10
  163.7 5.5 fusion.93
  169.2 22.1 %all-reduce.1 = (f32[640]{0:T(1024)S(1)}, f32[640]{0:T(1024)S(1)}) all-reduce(f32[640]{0:T(1024)S(1)} %bitcast.77, f32[640]{0:T(1024)S(1)} %bitcast.76), channel_id=1, replica_groups=mesh['rep'=2,'fs'=32,'tp'=2] {'tp'}, use_global_device_ids=true, to_apply=%region_4.5 | all-reduce | flops 1280 | bytes 10240 | tf_op jit(solution)/shard_map/psum | solution.py:84
  191.2 0.0 copy-done.9
  191.2 0.0 copy-done.10
  191.2 0.5 multiply_convert_fusion.1
  191.8 0.0 all-to-all-done.1
  191.8 3.1 convolution_convert_fusion
  194.9 0.3 copy.23
  195.2 5.8 all_to_all.21
  201.0 0.0 copy-start.2
  201.0 0.6 convert_reduce_fusion.1
  201.6 0.7 copy-done.2
  202.3 1.5 add_convert_fusion.1
  203.9 0.0 all-gather.7.cloned.1.call-update
  203.9 0.0 all-gather.11.cloned.1.call-start
  204.0 0.7 all-gather.11.cloned.1.call-update
  204.6 0.2 all-gather.9.cloned.1.call-start
  204.9 0.3 all-gather.9.cloned.1.call-update
  205.2 0.0 copy-start.11
  205.2 13.4 %all-gather.7.cloned.1.call-done = bf16[640,2048]{1,0:T(8,128)(2,1)} async-done(((bf16[640,1024]{1,0:T(8,128)(2,1)}), bf16[640,2048]{1,0:T(8,128)(2,1)}) %all-gather.7.cloned.1.call-update) | async-done | bytes 2621456 | tf_op jit(solution)/shard_map/all_gather | solution.py:95
  218.7 0.0 copy-start.3
  218.7 2.5 fusion
  221.2 190.3 %all-gather.11.cloned.1.call-done = bf16[4096,2048]{1,0:T(8,128)(2,1)} async-done(((bf16[128,2048]{1,0:T(8,128)(2,1)}), bf16[4096,2048]{1,0:T(8,128)(2,1)}) %all-gather.11.cloned.1.call-update) | async-done | bytes 16777232 | tf_op jit(solution)/shard_map/all_gather | solution.py:104
  411.5 222.9 %all-gather.9.cloned.1.call-done = bf16[2048,4096]{1,0:T(8,128)(2,1)} async-done(((bf16[2048,128]{1,0:T(8,128)(2,1)}), bf16[2048,4096]{1,0:T(8,128)(2,1)}) %all-gather.9.cloned.1.call-update) | async-done | bytes 16777232 | tf_op jit(solution)/shard_map/all_gather | solution.py:99
  634.4 0.0 copy-done.11
  634.4 0.0 copy-done.3
  634.4 33.8 %convolution_convert_fusion.1 = bf16[640,2048]{1,0:T(8,128)(2,1)} fusion(bf16[4096,2048]{1,0:T(8,128)(2,1)} %all-gather.11.cloned.1.call-done, bf16[2048,4096]{1,0:T(8,128)(2,1)} %all-gather.9.cloned.1.call-done, bf16[640,2048]{1,0:T(8,128)(2,1)S(1)} %copy-done.3, f32[2048]{0:T(1024)S(1)} %copy-done.11, f32[640]{0:T(1024)S(1)} %add_rsqrt_fusion), kind=kOutput, calls=%fused_computation.43 | convolution fusion | flops 21489254400 | bytes 38808064 | tf_op jit(solution)/shard_map/dot_general | solution.py:103
  668.2 2.0 copy.22
  670.2 29.3 %all_to_all.22 = bf16[2,640,1024]{2,1,0:T(8,128)(2,1)S(1)} all-to-all(bf16[2,640,1024]{2,1,0:T(8,128)(2,1)S(1)} %bitcast.71), channel_id=1, replica_groups=mesh['rep'=2,'fs'=32,'tp'=2] {'tp'}, dimensions={0} | all-to-all | bytes 5242880 | tf_op jit(solution)/shard_map/all_to_all | solution.py:41
  699.4 0.0 copy-start
  699.4 0.6 convert_reduce_fusion
  700.0 0.7 copy-done
  700.8 1.5 add_convert_fusion
  (5 shorter events, 0.1 us)
Async XLA Ops:
  6.5 151.2 %all-gather.5.cloned.1.call-start = ((), (), s32[]{:S(2)}) async-start(), calls=%async_computation.4 | async-start | bytes 4325376 | tf_op jit(solution)/shard_map/all_gather | solution.py:29
  10.0 7.0 copy-start.5
  18.6 173.2 %all-to-all-start.1 = ((bf16[32,512,64]{1,2,0:T(8,128)(2,1)}), bf16[32,512,64]{1,2,0:T(8,128)(2,1)}, u32[]{:S(2)}, u32[]{:S(2)}) async-start(bf16[32,512,64]{1,2,0:T(8,128)(2,1)} %broadcast_in_dim.5), calls=%async_computation.1 | async-start | bytes 4194304 | tf_op jit(solution)/shard_map/all_to_all | solution.py:12
  27.3 0.8 copy-start.6
  27.3 0.9 copy-start.7
  27.3 191.4 %all-gather.7.cloned.1.call-start = ((), (), s32[]{:S(2)}) async-start(), calls=%async_computation.5 | async-start | bytes 3932160 | tf_op jit(solution)/shard_map/all_gather | solution.py:95
  30.4 131.7 %copy-start.1 = (bf16[640,2048]{0,1:T(8,128)(2,1)S(1)}, bf16[640,2048]{0,1:T(8,128)(2,1)}, u32[]{:S(2)}) copy-start(bf16[640,2048]{0,1:T(8,128)(2,1)} %fusion.4) | copy-start | bytes 7864324
  157.8 4.3 copy-start.4
  162.0 1.6 copy-start.8
  163.7 27.6 %copy-start.9 = (f32[512]{0:T(512)S(1)}, f32[512]{0:T(512)}, u32[]{:S(2)}) copy-start(f32[512]{0:T(512)} %param.19) | copy-start | bytes 6148
  163.7 27.6 %copy-start.10 = (f32[512]{0:T(512)S(1)}, f32[512]{0:T(512)}, u32[]{:S(2)}) copy-start(f32[512]{0:T(512)} %param.18) | copy-start | bytes 6148
  201.0 1.3 copy-start.2
  203.9 207.6 %all-gather.11.cloned.1.call-start = ((), (), s32[]{:S(2)}) async-start(), calls=%async_computation.7 | async-start | bytes 17301504 | tf_op jit(solution)/shard_map/all_gather | solution.py:104
  204.6 429.8 %all-gather.9.cloned.1.call-start = ((), (), s32[]{:S(2)}) async-start(), calls=%async_computation.6 | async-start | bytes 17301504 | tf_op jit(solution)/shard_map/all_gather | solution.py:99
  205.2 429.2 %copy-start.11 = (f32[2048]{0:T(1024)S(1)}, f32[2048]{0:T(1024)}, u32[]{:S(2)}) copy-start(f32[2048]{0:T(1024)} %param.21) | copy-start | bytes 24580
  218.7 415.7 %copy-start.3 = (bf16[640,2048]{1,0:T(8,128)(2,1)S(1)}, bf16[640,2048]{1,0:T(8,128)(2,1)}, u32[]{:S(2)}) copy-start(bf16[640,2048]{1,0:T(8,128)(2,1)} %all-gather.7.cloned.1.call-done) | copy-start | bytes 7864324
  699.4 1.3 copy-start
Sparse Core Ops, SparseCore 0:
  9.0 148.7 all-gather.4
  204.0 14.6 all-gather.6
  220.3 191.0 all-gather.10
  412.9 221.4 all-gather.8
where the time goes:
time: 709 us
  waiting for transfers between devices  555 us (78%)
  blocking collectives  64.1 us (9%)
  matrix products  42.7 us (6%)
  other arithmetic  17 us (2%)
  between operations  13.3 us (2%)
  starting transfers between devices  8.94 us (1%)
  local copies, waits for them, and re-layouts  7.52 us (1%)
    all_gather x1, waiting for transfers between devices, shards(): lax.all_gather(w_up, 'fs', axis=1, tiled=True)  223 us
    all_gather x1, waiting for transfers between devices, shards(): lax.all_gather(w_down, 'fs', axis=0, tiled=True)  190 us
    all_gather x1, waiting for transfers between devices, side_by_side(): result = lax.all_gather(both, axis, axis=dim, tiled=True)  127 us
    all_to_all x2, blocking collectives, summed_on_arrival(): parts = lax.all_to_all(in_blocks(array, dim, count), axis, 0, 0, tiled=True)  35.1 us
    dot_general x1, matrix products, shards(): jnp.dot(hidden, lax.all_gather(w_down, 'fs', axis=0, tiled=True), preferr...  33.8 us
    psum x1, blocking collectives, shards(): lax.psum((jnp.sum(filtered, axis=1), jnp.sum(filtered * filtered, axis=1)...  22.1 us
  transfers between devices with their start and end apart: 5, of which 4 were waited for; matrix products, arithmetic and copies ran while one was open for 3% of the time, Pallas kernels for 0%

commit v1 on v0

--- a/solution.py
+++ b/solution.py
@@ -94,11 +94,10 @@
     second = (hidden_in.astype(jnp.float32) + summed).astype(jnp.bfloat16)
     gathered_feed = lax.all_gather(second, "tp", axis=1, tiled=True)
     normed_feed = rms_norm(gathered_feed, feed_gain)
-    up_proj = jnp.dot(
-        normed_feed,
-        lax.all_gather(w_up, "fs", axis=1, tiled=True),
-        preferred_element_type=jnp.float32,
+    clear_the_patch = lambda chunk, peer_axis: jnp.concatenate(
+        lax.all_gather(chunk, axis_name=peer_axis), axis=1
     )
+    up_proj = jnp.dot(normed_feed, clear_the_patch(w_up, "fs"), preferred_element_type=jnp.float32)
     hidden = jnp.square(jax.nn.relu(up_proj)).astype(jnp.bfloat16)
     feed_partial = jnp.dot(
         hidden, lax.all_gather(w_down, "fs", axis=0, tiled=True), preferred_element_type=jnp.float32

time: 709 us -> 635 us (0.90)
  waiting for transfers between devices: 555 us -> 485 us
  blocking collectives: 64.1 us -> 41.3 us
  local copies, waits for them, and re-layouts: 7.52 us -> 27.2 us
    all_gather x1, waiting for transfers between devices: 190 us -> 153 us  [shards(): lax.all_gather(w_down, 'fs', axis=0, tiled=True)]
    all_gather x1, waiting for transfers between devices: 223 us -> 190 us  [shards(): lax.all_gather(chunk, axis_name=peer_axis)]
    all_to_all x2, blocking collectives: 35.1 us -> 12.3 us  [summed_on_arrival(): parts = lax.all_to_all(in_blocks(array, dim, count), axis, 0, 0, tiled=True)]
    reshape x0 -> x1, local copies, waits for them, and re-layouts: none -> 21.5 us  [shards(): jnp.concatenate(lax.all_gather(chunk, axis_name=peer_axis), axis=1)]
    dot_general x1, matrix products: 33.8 us -> 16 us  [shards(): jnp.dot(hidden, lax.all_gather(w_down, 'fs', axis=0, tiled=True), preferr...]
    dot_general x0 -> x1, matrix products: none -> 16.3 us  [shards(): jnp.dot(normed_feed, clear_the_patch(w_up, 'fs'), preferred_element_type=...]
  transfers between devices with their start and end apart: 5 -> 5, of which waited for: 4 -> 4; matrix products, arithmetic and copies ran while one was open for 3% -> 9% of each run, Pallas kernels for 0% -> 0%
where the time goes in v1:
time: 635 us; the launch traced here: 634 us
  waiting for transfers between devices  485 us (76%)
  matrix products  41.4 us (7%)
  blocking collectives  41.3 us (7%)
  local copies, waits for them, and re-layouts  27.2 us (4%)
  other arithmetic  16.9 us (3%)
  between operations  13.3 us (2%)
  starting transfers between devices  8.94 us (1%)
    all_gather x1, waiting for transfers between devices, shards(): lax.all_gather(chunk, axis_name=peer_axis)  190 us
    all_gather x1, waiting for transfers between devices, shards(): lax.all_gather(w_down, 'fs', axis=0, tiled=True)  153 us
    all_gather x1, waiting for transfers between devices, side_by_side(): result = lax.all_gather(both, axis, axis=dim, tiled=True)  127 us
    psum x1, blocking collectives, shards(): lax.psum((jnp.sum(filtered, axis=1), jnp.sum(filtered * filtered, axis=1)...  22.1 us
    reshape x1, local copies, waits for them, and re-layouts, shards(): jnp.concatenate(lax.all_gather(chunk, axis_name=peer_axis), axis=1)  21.5 us
    dot_general x1, matrix products, shards(): jnp.dot(normed_feed, clear_the_patch(w_up, 'fs'), preferred_element_type=...  16.3 us
    dot_general x1, matrix products, shards(): jnp.dot(hidden, lax.all_gather(w_down, 'fs', axis=0, tiled=True), preferr...  16 us
    all_gather x1, waiting for transfers between devices, shards(): gathered_feed = lax.all_gather(second, 'tp', axis=1, tiled=True)  13.5 us
  transfers between devices with their start and end apart: 5, of which 4 were waited for; matrix products, arithmetic and copies ran while one was open for 9% of the time, Pallas kernels for 0%

profile of v1, /device:TPU:1, one launch (start us, length us, event | category | flops | bytes accessed | tf_op | source)
XLA Modules:
  0.0 634.3 jit_solution(14717275180474212320)
XLA Ops:
  6.5 0.0 all-gather.6.cloned.1.call-start
  6.5 1.5 pad_maximum_fusion
  8.1 0.0 all-gather.6.cloned.1.call-update
  8.1 1.7 copy.17
  9.8 0.2 broadcast_in_dim.4
  10.0 0.0 copy-start.5
  10.0 7.0 %all_to_all.20 = bf16[2,640,1024]{1,2,0:T(8,128)(2,1)S(1)} all-to-all(bf16[2,640,1024]{1,2,0:T(8,128)(2,1)S(1)} %broadcast_in_dim.4), channel_id=1, replica_groups=mesh['rep'=2,'fs'=32,'tp'=2] {'tp'}, dimensions={0} | all-to-all | bytes 5242880 | tf_op jit(solution)/shard_map/all_to_all | solution.py:12
  17.0 0.0 copy-done.5
  17.0 1.6 broadcast_in_dim.5
  18.6 8.6 %all-to-all-start.1 = ((bf16[32,512,64]{1,2,0:T(8,128)(2,1)}), bf16[32,512,64]{1,2,0:T(8,128)(2,1)}, u32[]{:S(2)}, u32[]{:S(2)}) async-start(bf16[32,512,64]{1,2,0:T(8,128)(2,1)} %broadcast_in_dim.5), calls=%async_computation.1 | async-start | bytes 4194304 | tf_op jit(solution)/shard_map/all_to_all | solution.py:12
  27.3 0.0 copy-start.6
  27.3 0.0 copy-start.7
  27.3 0.0 all-gather.8.cloned.1.call-start
  27.3 0.6 multiply_reduce_fusion
  27.9 0.2 copy-done.6
  28.2 0.0 copy-done.7
  28.2 2.2 fusion.4
  30.4 0.0 copy-start.1
  30.4 127.4 %all-gather.6.cloned.1.call-done = bf16[2048,1024]{1,0:T(8,128)(2,1)} async-done(((bf16[64,1024]{1,0:T(8,128)(2,1)}), bf16[2048,1024]{1,0:T(8,128)(2,1)}) %all-gather.6.cloned.1.call-update) | async-done | bytes 4194320 | tf_op jit(solution)/shard_map/all_gather | solution.py:29
  157.8 0.0 copy-start.4
  157.8 4.2 fusion.28
  162.0 0.0 copy-done.1
  162.0 0.0 copy-done.4
  162.0 0.0 copy-start.8
  162.1 1.6 fusion.16
  163.6 0.0 copy-done.8
  163.7 0.0 copy-start.9
  163.7 0.0 copy-start.10
  163.7 5.5 fusion.93
  169.2 22.1 %all-reduce.1 = (f32[640]{0:T(1024)S(1)}, f32[640]{0:T(1024)S(1)}) all-reduce(f32[640]{0:T(1024)S(1)} %bitcast.88, f32[640]{0:T(1024)S(1)} %bitcast.87), channel_id=1, replica_groups=mesh['rep'=2,'fs'=32,'tp'=2] {'tp'}, use_global_device_ids=true, to_apply=%region_4.5 | all-reduce | flops 1280 | bytes 10240 | tf_op jit(solution)/shard_map/psum | solution.py:84
  191.2 0.0 copy-done.9
  191.2 0.0 copy-done.10
  191.2 0.5 multiply_convert_fusion.1
  191.8 0.0 all-to-all-done.1
  191.8 3.1 convolution_convert_fusion
  194.9 0.3 copy.26
  195.2 5.8 all_to_all.21
  201.0 0.0 copy-start.2
  201.0 0.6 convert_reduce_fusion.1
  201.6 0.7 copy-done.2
  202.3 1.5 add_convert_fusion.1
  203.9 0.0 all-gather.8.cloned.1.call-update
  203.9 0.0 all-gather.12.cloned.1.call-start
  204.0 0.7 all-gather.12.cloned.1.call-update
  204.6 0.2 all-gather.10.cloned.1.call-start
  204.9 0.3 all-gather.10.cloned.1.call-update
  205.2 13.5 %all-gather.8.cloned.1.call-done = bf16[640,2048]{1,0:T(8,128)(2,1)} async-done(((bf16[640,1024]{1,0:T(8,128)(2,1)}), bf16[640,2048]{1,0:T(8,128)(2,1)}) %all-gather.8.cloned.1.call-update) | async-done | bytes 2621456 | tf_op jit(solution)/shard_map/all_gather | solution.py:95
  218.7 2.3 fusion
  221.0 190.5 %all-gather.12.cloned.1.call-done = bf16[65536,128]{1,0:T(8,128)(2,1)} async-done(((bf16[2048,128]{1,0:T(8,128)(2,1)}), bf16[65536,128]{1,0:T(8,128)(2,1)}) %all-gather.12.cloned.1.call-update) | async-done | bytes 16777232 | tf_op jit(solution)/shard_map/all_gather | solution.py:98
  411.5 0.0 copy-start.3
  411.5 0.0 copy-start.11
  411.5 21.5 %copy.19 = bf16[2048,32,128]{0,2,1:T(8,128)(2,1)} copy(bf16[2048,32,128]{2,0,1:T(8,128)(2,1)} %bitcast.79) | data formatting | bytes 33554432 | tf_op jit(solution)/shard_map/reshape | solution.py:97
  432.9 0.0 copy-done.3
  432.9 0.0 copy-done.11
  432.9 16.3 %multiply_convert_fusion.clone.4 = bf16[640,4096]{1,0:T(8,128)(2,1)} fusion(bf16[2048,4096]{0,1:T(8,128)(2,1)} %bitcast.80, bf16[640,2048]{1,0:T(8,128)(2,1)S(1)} %copy-done.3, f32[2048]{0:T(1024)S(1)} %copy-done.11, f32[640]{0:T(1024)S(1)} %add_rsqrt_fusion), kind=kOutput, calls=%fused_computation.clone.clone.clone.1 | convolution fusion | flops 10750525440 | bytes 24652288 | tf_op jit(solution)/shard_map/dot_general | solution.py:100
  449.3 152.8 %all-gather.10.cloned.1.call-done = bf16[4096,2048]{1,0:T(8,128)(2,1)} async-done(((bf16[128,2048]{1,0:T(8,128)(2,1)}), bf16[4096,2048]{1,0:T(8,128)(2,1)}) %all-gather.10.cloned.1.call-update) | async-done | bytes 16777232 | tf_op jit(solution)/shard_map/all_gather | solution.py:103
  602.1 16.0 %convolution_convert_fusion.1 = bf16[640,2048]{1,0:T(8,128)(2,1)S(1)} fusion(bf16[4096,2048]{1,0:T(8,128)(2,1)} %all-gather.10.cloned.1.call-done, bf16[640,4096]{1,0:T(8,128)(2,1)} %multiply_convert_fusion.clone.4), kind=kOutput, calls=%fused_computation.43 | convolution fusion | flops 10738728960 | bytes 24641536 | tf_op jit(solution)/shard_map/dot_general | solution.py:102
  618.1 0.3 copy.25
  618.4 6.5 %all_to_all.22 = bf16[2,640,1024]{2,1,0:T(8,128)(2,1)S(1)} all-to-all(bf16[2,640,1024]{2,1,0:T(8,128)(2,1)S(1)} %bitcast.82), channel_id=1, replica_groups=mesh['rep'=2,'fs'=32,'tp'=2] {'tp'}, dimensions={0} | all-to-all | bytes 5242880 | tf_op jit(solution)/shard_map/all_to_all | solution.py:41
  624.9 0.0 copy-start
  624.9 0.6 convert_reduce_fusion
  625.5 0.7 copy-done
  626.2 1.5 add_convert_fusion
  (5 shorter events, 0.1 us)
Async XLA Ops:
  6.5 151.2 %all-gather.6.cloned.1.call-start = ((), (), s32[]{:S(2)}) async-start(), calls=%async_computation.4 | async-start | bytes 4325376 | tf_op jit(solution)/shard_map/all_gather | solution.py:29
  10.0 7.0 %copy-start.5 = (bf16[512,64]{0,1:T(8,128)(2,1)S(1)}, bf16[512,64]{0,1:T(8,128)(2,1)}, u32[]{:S(2)}) copy-start(bf16[512,64]{0,1:T(8,128)(2,1)} %param.20) | copy-start | bytes 196612
  18.6 173.2 %all-to-all-start.1 = ((bf16[32,512,64]{1,2,0:T(8,128)(2,1)}), bf16[32,512,64]{1,2,0:T(8,128)(2,1)}, u32[]{:S(2)}, u32[]{:S(2)}) async-start(bf16[32,512,64]{1,2,0:T(8,128)(2,1)} %broadcast_in_dim.5), calls=%async_computation.1 | async-start | bytes 4194304 | tf_op jit(solution)/shard_map/all_to_all | solution.py:12
  27.3 0.8 copy-start.6
  27.3 0.9 copy-start.7
  27.3 191.4 %all-gather.8.cloned.1.call-start = ((), (), s32[]{:S(2)}) async-start(), calls=%async_computation.5 | async-start | bytes 3932160 | tf_op jit(solution)/shard_map/all_gather | solution.py:95
  30.4 131.7 %copy-start.1 = (bf16[640,2048]{0,1:T(8,128)(2,1)S(1)}, bf16[640,2048]{0,1:T(8,128)(2,1)}, u32[]{:S(2)}) copy-start(bf16[640,2048]{0,1:T(8,128)(2,1)} %fusion.4) | copy-start | bytes 7864324
  157.8 4.3 copy-start.4
  162.0 1.6 copy-start.8
  163.7 27.6 %copy-start.9 = (f32[512]{0:T(512)S(1)}, f32[512]{0:T(512)}, u32[]{:S(2)}) copy-start(f32[512]{0:T(512)} %param.19) | copy-start | bytes 6148
  163.7 27.6 %copy-start.10 = (f32[512]{0:T(512)S(1)}, f32[512]{0:T(512)}, u32[]{:S(2)}) copy-start(f32[512]{0:T(512)} %param.18) | copy-start | bytes 6148
  201.0 1.3 copy-start.2
  203.9 207.6 %all-gather.12.cloned.1.call-start = ((), (), s32[]{:S(2)}) async-start(), calls=%async_computation.7 | async-start | bytes 17301504 | tf_op jit(solution)/shard_map/all_gather | solution.py:98
  204.6 397.4 %all-gather.10.cloned.1.call-start = ((), (), s32[]{:S(2)}) async-start(), calls=%async_computation.6 | async-start | bytes 17301504 | tf_op jit(solution)/shard_map/all_gather | solution.py:103
  411.5 21.5 %copy-start.3 = (bf16[640,2048]{1,0:T(8,128)(2,1)S(1)}, bf16[640,2048]{1,0:T(8,128)(2,1)}, u32[]{:S(2)}) copy-start(bf16[640,2048]{1,0:T(8,128)(2,1)} %all-gather.8.cloned.1.call-done) | copy-start | bytes 7864324
  411.5 21.5 %copy-start.11 = (f32[2048]{0:T(1024)S(1)}, f32[2048]{0:T(1024)}, u32[]{:S(2)}) copy-start(f32[2048]{0:T(1024)} %param.21) | copy-start | bytes 24580
  624.9 1.3 copy-start
Sparse Core Ops, SparseCore 0:
  9.0 148.7 all-gather.5
  204.0 14.6 all-gather.7
  220.3 191.0 all-gather.11
  413.0 189.0 all-gather.9
